TPU v7x, 32 devices: a whole 2x2x4 slice. The times are simulated.
32 devices in a mesh: grp: 2 (over y), sp: 4 (over z), tp: 4 (over x, core).
Axes of the slice: x: 2, y: 2, z: 4, core: 2. Of those that a mesh axis runs over, the one named last changes fastest.
Arguments:
- conv_input: bfloat16 [4096, 1024], P(('grp', 'sp'), 'tp'), parts along dimension 0, may hold values from -6 to 6
- pre_gate: bfloat16 [4096, 1024], P(('grp', 'sp'), 'tp'), parts along dimension 0, may hold values from -6 to 6
- post_gate: bfloat16 [4096, 1024], P(('grp', 'sp'), 'tp'), parts along dimension 0, may hold values from -6 to 6
- conv_taps: float32 [3, 1024], replicated, may hold values from -3.5 to 3.5
- out_proj: bfloat16 [1024, 2048], replicated, may hold values from -0.1875 to 0.1875
- residual_in: bfloat16 [4096, 2048], P(('grp', 'sp', 'tp')), parts along dimension 0, may hold values from -6 to 6
- norm_gain: float32 [2048], replicated, may hold values from 0.1 to 1.9
- routes: int32 [4096, 2], P(('grp', 'sp', 'tp')), parts along dimension 0, may hold values from 0 to 7, as said below
- route_weight: float32 [4096, 2], P(('grp', 'sp', 'tp')), parts along dimension 0, may hold values from 0.1 to 1
- w_gate: bfloat16 [8, 2048, 1024], P('sp', None, 'tp'), may hold values from -0.125 to 0.125
- w_up: bfloat16 [8, 2048, 1024], P('sp', None, 'tp'), may hold values from -0.125 to 0.125
- w_down: bfloat16 [8, 1024, 2048], P('sp', 'tp'), may hold values from -0.1875 to 0.1875
Outputs:
- layer_out: bfloat16 [4096, 2048], P(('grp', 'sp', 'tp')), parts along dimension 0
There are 2 independent parts, one for each index of `grp`. A program takes and returns all parts, laid end to end along the dimension named above; an argument that names none is the same for every part. Nothing has to cross between parts.
Inputs may be any that keep to these rules, and one draw needn't show every extreme that they name: `routes`: the two numbers of a row differ and lie in the same group of 2 consecutive experts. In each aligned block of 128 rows every expert is named exactly 32 times.
All inputs are finite; a program needn't handle non-finite values.
Results may differ from a plain program's by a relative error of at most 0.0085.
Values may be sent and summed in bfloat16 or wider, within the bound.
No kernel may reach another device: no remote copies, remote signals or barrier semaphores. Data moves between devices by JAX's collectives and lax.ppermute only.
A program may use at most 64 MiB of HBM per device.

v0:
```python
import jax
import jax.numpy as jnp
from jax import lax
from jax.sharding import PartitionSpec as P


def shifted(block, axis, distance):
    devices = range(lax.axis_size(axis))
    route = [(i - distance, i) for i in devices if i - distance in devices]
    return lax.ppermute(block, axis, route)


def on_device(
    conv_input,
    pre_gate,
    post_gate,
    conv_taps,
    out_proj,
    residual_in,
    norm_gain,
    routes,
    route_weight,
    w_gate,
    w_up,
    w_down,
):
    shards = lax.axis_size("tp")
    place = lax.axis_index("tp")
    seq_ranks = lax.axis_size("sp")
    channels = conv_input.shape[1]
    width = residual_in.shape[1]
    taps = lax.dynamic_slice_in_dim(conv_taps, place * channels, channels, 1)
    prior_input, prior_gate = shifted((conv_input[-2:], pre_gate[-2:]), "sp", 1)
    gated = jnp.concatenate(
        [
            prior_gate.astype(jnp.float32) * prior_input.astype(jnp.float32),
            pre_gate.astype(jnp.float32) * conv_input.astype(jnp.float32),
        ],
        axis=0,
    )
    conv = gated[2:] * taps[2] + gated[1:-1] * taps[1] + gated[:-2] * taps[0]
    mixed = (post_gate.astype(jnp.float32) * conv).astype(jnp.bfloat16)
    token_rows = lax.all_to_all(mixed, "tp", split_axis=0, concat_axis=1, tiled=True)
    projected = jnp.dot(token_rows, out_proj, preferred_element_type=jnp.float32)
    stream = residual_in.astype(jnp.float32) + projected
    scale = lax.rsqrt(jnp.mean(stream * stream, axis=-1, keepdims=True) + 1e-06)
    normed = (stream * scale * norm_gain).astype(jnp.bfloat16)
    block_rows = routes.shape[0]
    local_experts = w_gate.shape[0]
    experts = local_experts * seq_ranks
    capacity = 2 * block_rows // experts
    flat_routes = routes.reshape(-1)
    position = jnp.arange(flat_routes.shape[0], dtype=jnp.int32)
    earlier = (flat_routes[:, None] == flat_routes[None, :]) & (
        position[None, :] < position[:, None]
    )
    rank = jnp.sum(earlier.astype(jnp.int32), axis=1)
    slot = flat_routes * capacity + rank
    outgoing = (
        jnp.zeros((experts * capacity, width), jnp.bfloat16).at[slot].set(normed[position // 2])
    )
    outgoing = outgoing.reshape(seq_ranks, local_experts, capacity, width)
    spread = lax.all_gather(
        lax.all_to_all(outgoing, "sp", split_axis=0, concat_axis=0, tiled=True)[:, None],
        "tp",
        axis=1,
        tiled=True,
    )
    count = spread.shape[3]
    partials = []
    for expert in range(local_experts):
        rows = spread[:, :, expert].reshape(seq_ranks * shards * count, width)
        gate = jnp.dot(rows, w_gate[expert], preferred_element_type=jnp.float32)
        upper = jnp.dot(rows, w_up[expert], preferred_element_type=jnp.float32)
        hidden = (jax.nn.silu(gate) * upper).astype(jnp.bfloat16)
        part = jnp.dot(hidden, w_down[expert], preferred_element_type=jnp.float32).astype(
            jnp.bfloat16
        )
        partials.append(part.reshape(seq_ranks, shards, count, width))
    stacked = jnp.stack(partials, axis=2)
    summed = lax.psum_scatter(stacked, "tp", scatter_dimension=1, tiled=True).astype(jnp.float32)
    returned = lax.all_to_all(
        summed[:, 0].astype(jnp.bfloat16), "sp", split_axis=0, concat_axis=0, tiled=True
    )
    results = returned.reshape(experts * capacity, width)[slot]
    results = results.reshape(block_rows, 2, width).astype(jnp.float32)
    weighted = jnp.sum(route_weight[:, :, None] * results, axis=1)
    return (stream + weighted).astype(jnp.bfloat16)


def solution(mesh):
    return jax.shard_map(
        on_device,
        mesh=mesh,
        in_specs=(
            P(("grp", "sp"), "tp"),
            P(("grp", "sp"), "tp"),
            P(("grp", "sp"), "tp"),
            P(),
            P(),
            P(("grp", "sp", "tp"), None),
            P(),
            P(("grp", "sp", "tp"), None),
            P(("grp", "sp", "tp"), None),
            P("sp", None, "tp"),
            P("sp", None, "tp"),
            P("sp", "tp", None),
        ),
        out_specs=P(("grp", "sp", "tp"), None),
        check_vma=False,
    )
```

profile of v0, /device:TPU:0, one launch (start us, length us, event | category | flops | bytes accessed | tf_op | source)
XLA Modules:
  0.0 258.8 jit_solution(13987586749709506822)
XLA Ops:
  6.5 0.0 copy-start.1
  6.5 0.7 slice.46
  7.3 4.9 %collective-permute-start = (bf16[2,256]{1,0:T(2,128)(2,1)S(1)}, bf16[2,256]{1,0:T(2,128)(2,1)S(1)}, u32[]{:S(2)}, u32[]{:S(2)}) collective-permute-start(bf16[2,256]{1,0:T(2,128)(2,1)S(1)} %slice.46), channel_id=1, source_target_pairs={{0,4},{4,8},{8,12},{1,5},{5,9},{9,13},{2,6},{6,10},{10,14},{3,7},{... | collective-permute-start | bytes 3080 | tf_op jit(solution)/shard_map/ppermute | solution.py:10
  12.2 0.7 slice.47
  12.9 3.5 %collective-permute-start.1 = (bf16[2,256]{1,0:T(2,128)(2,1)S(1)}, bf16[2,256]{1,0:T(2,128)(2,1)S(1)}, u32[]{:S(2)}, u32[]{:S(2)}) collective-permute-start(bf16[2,256]{1,0:T(2,128)(2,1)S(1)} %slice.47), channel_id=1, source_target_pairs={{0,4},{4,8},{8,12},{1,5},{5,9},{9,13},{2,6},{6,10},{10,14},{3,7},{... | collective-permute-start | bytes 3080 | tf_op jit(solution)/shard_map/ppermute | solution.py:10
  16.4 1.1 convert_multiply_fusion
  17.5 0.8 copy.32
  18.3 0.7 broadcast_multiply_fusion
  19.0 0.1 eq.15
  19.1 0.2 convert_reduce_fusion
  19.3 0.9 fusion.46
  20.2 0.1 copy.31
  20.3 0.1 mul.114
  20.5 0.0 collective-permute-done
  20.5 0.0 collective-permute-done.1
  20.5 1.9 fusion.27
  22.4 3.4 %all-to-all-start = ((bf16[4,128,256]{2,1,0:T(8,128)(2,1)}), bf16[4,128,256]{2,1,0:T(8,128)(2,1)S(1)}, u32[]{:S(2)}, u32[]{:S(2)}) async-start(bf16[4,128,256]{2,1,0:T(8,128)(2,1)} %bitcast.3), calls=%async_computation | async-start | bytes 524288 | tf_op jit(solution)/shard_map/all_to_all | solution.py:43
  25.8 0.0 all-gather.3.cloned.1.call-start
  25.8 5.9 %all-to-all-done = bf16[4,128,256]{2,1,0:T(8,128)(2,1)S(1)} async-done(((bf16[4,128,256]{2,1,0:T(8,128)(2,1)}), bf16[4,128,256]{2,1,0:T(8,128)(2,1)S(1)}, u32[]{:S(2)}, u32[]{:S(2)}) %all-to-all-start) | async-done | bytes 262176 | tf_op jit(solution)/shard_map/all_to_all | solution.py:43
  31.7 0.2 copy.29
  31.9 0.0 copy-done.1
  31.9 0.0 copy-start.2
  31.9 3.0 %multiply_reduce_fusion.1 = (f32[128]{0:T(128)S(1)}, f32[128,2048]{1,0:T(8,128)S(1)}) fusion(bf16[128,1024]{0,1:T(8,128)(2,1)S(1)} %bitcast.62, bf16[1024,2048]{1,0:T(8,128)(2,1)} %param.16, bf16[128,2048]{1,0:T(8,128)(2,1)S(1)} %copy-done.1), kind=kOutput, calls=%fused_computation.31 | convolution fusion | flops 537919360 | bytes 6029824 | tf_op jit(solution)/shard_map/dot_general | solution.py:44
  35.0 0.0 copy-done.2
  35.0 0.2 multiply_convert_fusion
  35.1 5.7 %scatter_custom_fusion = bf16[256,2048]{1,0:T(8,128)(2,1)S(1)} fusion(s32[256]{0:T(256)S(1)} %bitcast.67, bf16[128,2048]{1,0:T(8,128)(2,1)S(1)} %multiply_convert_fusion, s32[1024]{0:T(1024)S(1)} %pad_clamp_fusion.1, bf16[]{:T(256)} %constant.35.clone.1), kind=kCustom, calls=%fused_computation.21 | custom fusion | bytes 1048578 | tf_op jit(solution)/shard_map/scatter | solution.py:60
  40.8 28.9 %all_to_all.29 = bf16[4,2,32,2048]{3,2,1,0:T(8,128)(2,1)} all-to-all(bf16[4,2,32,2048]{3,2,1,0:T(8,128)(2,1)S(1)} %bitcast.55), channel_id=1, replica_groups=mesh['grp'=2,'sp'=4,'tp'=4] {'sp'}, dimensions={0} | all-to-all | bytes 2097152 | tf_op jit(solution)/shard_map/all_to_all | solution.py:64
  69.7 0.0 all-gather.3.cloned.1.call-update
  69.7 0.2 all-reduce.3.cloned.1.call-start
  70.0 32.8 %all-gather.3.cloned.1.call-done = bf16[4,8,32,2048]{3,2,1,0:T(8,128)(2,1)} async-done(((bf16[4,2,32,2048]{3,2,1,0:T(8,128)(2,1)}), bf16[4,8,32,2048]{3,2,1,0:T(8,128)(2,1)}) %all-gather.3.cloned.1.call-update) | async-done | bytes 4194320 | tf_op jit(solution)/shard_map/all_gather | solution.py:63
  102.7 0.0 copy-start.4
  102.7 2.8 %fusion.45 = (bf16[4,4,1,32,2048]{4,3,2,1,0:T(8,128)(2,1)S(1)}, bf16[4,4,1,32,2048]{4,3,2,1,0:T(8,128)(2,1)S(1)}) fusion(bf16[4,4,2,32,2048]{4,3,2,1,0:T(8,128)(2,1)} %bitcast.54), kind=kLoop, calls=%fused_computation.73 | loop fusion | bytes 8388608 | tf_op jit(solution)/shard_map/slice | solution.py:72
  105.5 0.0 copy-start
  105.5 0.1 copy-done.4
  105.6 1.5 fusion.10
  107.1 0.0 copy-done
  107.1 1.5 fusion.5
  108.6 6.0 %convolution_convert_fusion.1 = bf16[512,2048]{1,0:T(8,128)(2,1)} fusion(bf16[512,2048]{1,0:T(8,128)(2,1)} %bitcast.59, bf16[2,256,2048]{2,1,0:T(8,128)(2,1)} %param.23, bf16[2,2048,256]{2,1,0:T(8,128)(2,1)} %param.22, f32[512,256]{1,0:T(8,128)} %fusion.10), kind=kOutput, calls=%fused_computation.5 | convolution fusion | flops 1075576832 | bytes 6815744 | tf_op jit(solution)/shard_map/dot_general | solution.py:76
  114.5 5.4 %convolution_convert_fusion = bf16[512,2048]{1,0:T(8,128)(2,1)} fusion(bf16[512,2048]{1,0:T(8,128)(2,1)S(1)} %bitcast.57, bf16[2,256,2048]{2,1,0:T(8,128)(2,1)} %param.23, bf16[2,2048,256]{2,1,0:T(8,128)(2,1)} %param.22, f32[512,256]{1,0:T(8,128)} %fusion.5), kind=kOutput, calls=%fused_computation.4 | convolution fusion | flops 1075576832 | bytes 6815744 | tf_op jit(solution)/shard_map/dot_general | solution.py:76
  119.9 4.5 %pad_maximum_fusion = bf16[4,4,2,32,2048]{4,3,1,0,2:T(8,128)(2,1)} fusion(bf16[4,4,1,32,2048]{4,3,1,0,2:T(8,128)(2,1)} %bitcast.61, bf16[4,4,1,32,2048]{4,3,1,0,2:T(8,128)(2,1)} %bitcast.60), kind=kLoop, calls=%fused_computation.3 | loop fusion | flops 2097152 | bytes 8388608 | tf_op jit(solution)/shard_map/stack | solution.py:80
  124.5 0.0 copy-start.5
  124.5 0.0 all-reduce.3.cloned.1.call-update
  124.5 0.6 copy-done.5
  125.1 0.6 dynamic-slice
  125.7 84.4 %all-reduce.3.cloned.1.call-done = bf16[4,4,2,32,2048]{4,3,1,0,2:T(8,128)(2,1)} async-done(((bf16[4,4,2,32,2048]{4,3,1,0,2:T(8,128)(2,1)}), bf16[4,4,2,32,2048]{4,3,1,0,2:T(8,128)(2,1)}) %all-reduce.3.cloned.1.call-update) | async-done | bytes 4194320
  210.1 1.9 dynamic-slice_bitcast_fusion
  212.1 0.0 copy-start.3
  212.1 1.0 copy.33
  213.1 4.6 %all-to-all-start.2 = ((bf16[4,2,32,2048]{3,2,1,0:T(8,128)(2,1)}), bf16[4,2,32,2048]{3,2,1,0:T(8,128)(2,1)S(1)}, u32[]{:S(2)}, u32[]{:S(2)}) async-start(bf16[4,2,32,2048]{3,2,1,0:T(8,128)(2,1)} %copy.33), calls=%async_computation.2 | async-start | bytes 2097152 | tf_op jit(solution)/shard_map/all_to_all | solution.py:82
  217.7 0.0 copy-done.3
  217.7 0.1 copy.30
  217.8 25.3 %all-to-all-done.2 = bf16[4,2,32,2048]{3,2,1,0:T(8,128)(2,1)S(1)} async-done(((bf16[4,2,32,2048]{3,2,1,0:T(8,128)(2,1)}), bf16[4,2,32,2048]{3,2,1,0:T(8,128)(2,1)S(1)}, u32[]{:S(2)}, u32[]{:S(2)}) %all-to-all-start.2) | async-done | bytes 1048608 | tf_op jit(solution)/shard_map/all_to_all | solution.py:82
  243.1 2.3 gather_fusion
  245.5 2.4 reshape.99
  247.8 3.2 %multiply_reduce_fusion = f32[128,2048]{1,0:T(8,128)S(1)} fusion(f32[128,2,2048]{2,1,0:T(2,128)S(1)} %reshape.99, f32[128,2]{1,0:T(8,128)S(1)} %copy.30), kind=kLoop, calls=%fused_computation.7 | loop fusion | flops 786432 | bytes 3146752 | tf_op jit(solution)/shard_map/reduce_sum | solution.py:87
  251.0 0.9 add_convert_fusion
  (6 shorter events, 0.0 us)
Async XLA Ops:
  6.5 25.4 %copy-start.1 = (bf16[128,2048]{1,0:T(8,128)(2,1)S(1)}, bf16[128,2048]{1,0:T(8,128)(2,1)}, u32[]{:S(2)}) copy-start(bf16[128,2048]{1,0:T(8,128)(2,1)} %param.17) | copy-start | bytes 1572868
  7.3 13.2 %collective-permute-start = (bf16[2,256]{1,0:T(2,128)(2,1)S(1)}, bf16[2,256]{1,0:T(2,128)(2,1)S(1)}, u32[]{:S(2)}, u32[]{:S(2)}) collective-permute-start(bf16[2,256]{1,0:T(2,128)(2,1)S(1)} %slice.46), channel_id=1, source_target_pairs={{0,4},{4,8},{8,12},{1,5},{5,9},{9,13},{2,6},{6,10},{10,14},{3,7},{... | collective-permute-start | bytes 3080 | tf_op jit(solution)/shard_map/ppermute | solution.py:10
  12.9 7.5 %collective-permute-start.1 = (bf16[2,256]{1,0:T(2,128)(2,1)S(1)}, bf16[2,256]{1,0:T(2,128)(2,1)S(1)}, u32[]{:S(2)}, u32[]{:S(2)}) collective-permute-start(bf16[2,256]{1,0:T(2,128)(2,1)S(1)} %slice.47), channel_id=1, source_target_pairs={{0,4},{4,8},{8,12},{1,5},{5,9},{9,13},{2,6},{6,10},{10,14},{3,7},{... | collective-permute-start | bytes 3080 | tf_op jit(solution)/shard_map/ppermute | solution.py:10
  22.4 9.4 %all-to-all-start = ((bf16[4,128,256]{2,1,0:T(8,128)(2,1)}), bf16[4,128,256]{2,1,0:T(8,128)(2,1)S(1)}, u32[]{:S(2)}, u32[]{:S(2)}) async-start(bf16[4,128,256]{2,1,0:T(8,128)(2,1)} %bitcast.3), calls=%async_computation | async-start | bytes 524288 | tf_op jit(solution)/shard_map/all_to_all | solution.py:43
  25.8 76.9 %all-gather.3.cloned.1.call-start = ((), (), s32[]{:S(2)}) async-start(), calls=%async_computation.3 | async-start | bytes 5242880 | tf_op jit(solution)/shard_map/all_gather | solution.py:63
  31.9 3.0 %copy-start.2 = (f32[2048]{0:T(1024)S(1)}, f32[2048]{0:T(1024)}, u32[]{:S(2)}) copy-start(f32[2048]{0:T(1024)} %param.18) | copy-start | bytes 24580
  69.7 140.4 %all-reduce.3.cloned.1.call-start = ((), (), s32[]{:S(2)}) async-start(), calls=%async_computation.4 | async-start | bytes 8388608
  102.7 2.9 %copy-start.4 = (bf16[2,2048,256]{2,1,0:T(8,128)(2,1)S(1)}, bf16[2,2048,256]{2,1,0:T(8,128)(2,1)}, u32[]{:S(2)}) copy-start(bf16[2,2048,256]{2,1,0:T(8,128)(2,1)} %param.21) | copy-start | bytes 6291460
  105.5 1.6 copy-start
  124.5 0.7 copy-start.5
  212.1 5.6 %copy-start.3 = (f32[128,2]{0,1:T(2,128)S(1)}, f32[128,2]{0,1:T(2,128)}, u32[]{:S(2)}) copy-start(f32[128,2]{0,1:T(2,128)} %param.20) | copy-start | bytes 3076
  213.1 30.0 %all-to-all-start.2 = ((bf16[4,2,32,2048]{3,2,1,0:T(8,128)(2,1)}), bf16[4,2,32,2048]{3,2,1,0:T(8,128)(2,1)S(1)}, u32[]{:S(2)}, u32[]{:S(2)}) async-start(bf16[4,2,32,2048]{3,2,1,0:T(8,128)(2,1)} %copy.33), calls=%async_computation.2 | async-start | bytes 2097152 | tf_op jit(solution)/shard_map/all_to_all | solution.py:82
Sparse Core Ops, SparseCore 0:
  69.8 32.8 all-gather.2
  124.6 85.4 all-reduce.2
where the time goes:
time: 259 us
  waiting for transfers between devices  148 us (57%)
  blocking collectives  28.9 us (11%)
  local copies, waits for them, and re-layouts  21.2 us (8%)
  matrix products  17.4 us (7%)
  starting transfers between devices  16.7 us (6%)
  between operations  13.6 us (5%)
  other arithmetic  12.7 us (5%)
    unnamed x3, waiting for transfers between devices  84.5 us
    all_gather x1, waiting for transfers between devices, on_device(): lax.all_gather(lax.all_to_all(outgoing, 'sp', split_axis=0, concat_axis=0...  32.8 us
    all_to_all x1, blocking collectives, on_device(): lax.all_to_all(outgoing, 'sp', split_axis=0, concat_axis=0, tiled=True)  28.9 us
    all_to_all x1, waiting for transfers between devices, on_device(): lax.all_to_all(summed[:, 0].astype(jnp.bfloat16), 'sp', split_axis=0, con...  25.3 us
    dot_general x2, matrix products, on_device(): jnp.dot(hidden, w_down[expert], preferred_element_type=jnp.float32)  11.3 us
    ppermute x2, starting transfers between devices, shifted(): return lax.ppermute(block, axis, route)  8.42 us
    all_to_all x1, waiting for transfers between devices, on_device(): lax.all_to_all(mixed, 'tp', split_axis=0, concat_axis=1, tiled=True)  5.91 us
    scatter x1, local copies, waits for them, and re-layouts, on_device(): jnp.zeros((experts * capacity, width), jnp.bfloat16).at[slot]  5.7 us
  transfers between devices with their start and end apart: 6, of which 4 were waited for; matrix products, arithmetic and copies ran while one was open for 2% of the time, Pallas kernels for 0%

commit v1 on v0

--- a/solution.py
+++ b/solution.py
@@ -2,6 +2,9 @@
 import jax.numpy as jnp
 from jax import lax
 from jax.sharding import PartitionSpec as P
+
+GROUPS = 4
+LANES = 128
 
 
 def shifted(block, axis, distance):
@@ -10,27 +13,16 @@
     return lax.ppermute(block, axis, route)
 
 
-def on_device(
-    conv_input,
-    pre_gate,
-    post_gate,
-    conv_taps,
-    out_proj,
-    residual_in,
-    norm_gain,
-    routes,
-    route_weight,
-    w_gate,
-    w_up,
-    w_down,
-):
-    shards = lax.axis_size("tp")
-    place = lax.axis_index("tp")
-    seq_ranks = lax.axis_size("sp")
+def flipped(block, axis, bit):
+    return lax.ppermute(block, axis, [(i, i ^ bit) for i in range(lax.axis_size(axis))])
+
+
+def mix(conv_input, pre_gate, post_gate, conv_taps):
     channels = conv_input.shape[1]
-    width = residual_in.shape[1]
-    taps = lax.dynamic_slice_in_dim(conv_taps, place * channels, channels, 1)
-    prior_input, prior_gate = shifted((conv_input[-2:], pre_gate[-2:]), "sp", 1)
+    taps = lax.dynamic_slice_in_dim(conv_taps, lax.axis_index("tp") * channels, channels, 1)
+    edge = jnp.concatenate([conv_input[-2:], pre_gate[-2:]], axis=1)
+    prior = shifted(edge, "sp", 1)
+    prior_input, prior_gate = prior[:, :channels], prior[:, channels:]
     gated = jnp.concatenate(
         [
             prior_gate.astype(jnp.float32) * prior_input.astype(jnp.float32),
@@ -39,13 +31,75 @@
         axis=0,
     )
     conv = gated[2:] * taps[2] + gated[1:-1] * taps[1] + gated[:-2] * taps[0]
-    mixed = (post_gate.astype(jnp.float32) * conv).astype(jnp.bfloat16)
+    return (post_gate.astype(jnp.float32) * conv).astype(jnp.bfloat16)
+
+
+def project(mixed, out_proj, residual_in, norm_gain):
     token_rows = lax.all_to_all(mixed, "tp", split_axis=0, concat_axis=1, tiled=True)
     projected = jnp.dot(token_rows, out_proj, preferred_element_type=jnp.float32)
     stream = residual_in.astype(jnp.float32) + projected
     scale = lax.rsqrt(jnp.mean(stream * stream, axis=-1, keepdims=True) + 1e-06)
     normed = (stream * scale * norm_gain).astype(jnp.bfloat16)
-    block_rows = routes.shape[0]
+    return stream, normed
+
+
+def route_by_group(stream, normed, routes, route_weight, w_gate, w_up, w_down):
+    shards = lax.axis_size("tp")
+    seq_ranks = lax.axis_size("sp")
+    block_rows, width = stream.shape
+    local_experts = w_gate.shape[0]
+    capacity = block_rows // seq_ranks
+    group = routes[:, 0] // local_experts
+    order = jnp.arange(block_rows, dtype=jnp.int32)
+    earlier = (group[:, None] == group[None, :]) & (order[None, :] < order[:, None])
+    slot = group * capacity + jnp.sum(earlier.astype(jnp.int32), axis=1)
+    select = (order[:, None] == slot[None, :]).astype(jnp.bfloat16)
+    member = routes[:, :, None] % local_experts == jnp.arange(local_experts, dtype=jnp.int32)
+    weight = jnp.sum(jnp.where(member, route_weight[:, :, None], 0.0), axis=1)
+    high = lax.reduce_precision(weight, 8, 7)
+    labels = jnp.concatenate([high, weight - high], axis=1).astype(jnp.bfloat16)
+    labels = jnp.pad(labels, ((0, 0), (0, LANES - labels.shape[1])))
+    rows = jnp.concatenate([normed, labels], axis=1)
+    outgoing = jnp.dot(select, rows, preferred_element_type=jnp.float32).astype(jnp.bfloat16)
+    outgoing = outgoing.reshape(seq_ranks, capacity, width + LANES)
+    arrived = lax.all_to_all(outgoing, "sp", split_axis=0, concat_axis=0, tiled=True)
+    blocks = {0: arrived.reshape(block_rows, width + LANES)}
+    bits = [1 << b for b in range(shards.bit_length() - 1)]
+    for bit in reversed(bits):
+        blocks.update({k | bit: flipped(v, "tp", bit) for k, v in blocks.items()})
+    down = w_down.reshape(local_experts * w_down.shape[1], width)
+    parts = {}
+    for k, block in blocks.items():
+        features = block[:, :width]
+        marks = block[:, width:].astype(jnp.float32)
+        hidden = []
+        for expert in range(local_experts):
+            gate = jnp.dot(features, w_gate[expert], preferred_element_type=jnp.float32)
+            upper = jnp.dot(features, w_up[expert], preferred_element_type=jnp.float32)
+            scale = marks[:, expert] + marks[:, local_experts + expert]
+            hidden.append((jax.nn.silu(gate) * upper * scale[:, None]).astype(jnp.bfloat16))
+        hidden = jnp.concatenate(hidden, axis=1)
+        parts[k] = jnp.dot(hidden, down, preferred_element_type=jnp.float32)
+    for bit in bits:
+        for k in [k for k in parts if k & bit]:
+            parts[k ^ bit] += flipped(parts.pop(k).astype(jnp.bfloat16), "tp", bit).astype(
+                jnp.float32
+            )
+    summed = parts[0].astype(jnp.bfloat16).reshape(seq_ranks, capacity, width)
+    returned = lax.all_to_all(summed, "sp", split_axis=0, concat_axis=0, tiled=True)
+    weighted = lax.dot_general(
+        select,
+        returned.reshape(block_rows, width),
+        (((0,), (0,)), ((), ())),
+        preferred_element_type=jnp.float32,
+    )
+    return (stream + weighted).astype(jnp.bfloat16)
+
+
+def route_by_expert(stream, normed, routes, route_weight, w_gate, w_up, w_down):
+    shards = lax.axis_size("tp")
+    seq_ranks = lax.axis_size("sp")
+    block_rows, width = stream.shape
     local_experts = w_gate.shape[0]
     experts = local_experts * seq_ranks
     capacity = 2 * block_rows // experts
@@ -88,6 +142,28 @@
     return (stream + weighted).astype(jnp.bfloat16)
 
 
+def on_device(
+    conv_input,
+    pre_gate,
+    post_gate,
+    conv_taps,
+    out_proj,
+    residual_in,
+    norm_gain,
+    routes,
+    route_weight,
+    w_gate,
+    w_up,
+    w_down,
+):
+    shards = lax.axis_size("tp")
+    mixed = mix(conv_input, pre_gate, post_gate, conv_taps)
+    stream, normed = project(mixed, out_proj, residual_in, norm_gain)
+    whole_groups = lax.axis_size("sp") == GROUPS and shards & (shards - 1) == 0
+    route = route_by_group if whole_groups else route_by_expert
+    return route(stream, normed, routes, route_weight, w_gate, w_up, w_down)
+
+
 def solution(mesh):
     return jax.shard_map(
         on_device,

time: 259 us -> 97.7 us (0.38)
  waiting for transfers between devices: 148 us -> 28.6 us
  local copies, waits for them, and re-layouts: 21.2 us -> 2.75 us
  between operations: 13.6 us -> 0.34 us
  blocking collectives: 28.9 us -> 35.7 us
  matrix products: 17.4 us -> 11.4 us
  other arithmetic: 12.7 us -> 7.07 us
  starting transfers between devices: 16.7 us -> 11.3 us
    unnamed x3 -> x0, waiting for transfers between devices: 84.5 us -> none
    all_gather x1 -> x0, waiting for transfers between devices: 32.8 us -> none  [on_device(): lax.all_gather(lax.all_to_all(outgoing, 'sp', split_axis=0, concat_axis=0...]
    all_to_all x2 -> x1, waiting for transfers between devices: 31.2 us -> 5.94 us  [project(): lax.all_to_all(mixed, 'tp', split_axis=0, concat_axis=1, tiled=True)]
    ppermute x0 -> x6, waiting for transfers between devices: none -> 22.7 us  [flipped(): lax.ppermute(block, axis, [(i, i ^ bit) for i in range(lax.axis_size(axis...]
    all_to_all x1 -> x2, blocking collectives: 28.9 us -> 35.7 us  [the longest x1 18.7 us: route_by_group(): lax.all_to_all(outgoing, 'sp', split_axis=0, concat_axis=0, tiled=True)]
    dot_general x5 -> x23, matrix products: 17.4 us -> 11.4 us  [the longest x1 3.01 us: project(): jnp.dot(token_rows, out_proj, preferred_element_type=jnp.float32)]
    scatter x1 -> x0, local copies, waits for them, and re-layouts: 5.7 us -> none  [on_device(): jnp.zeros((experts * capacity, width), jnp.bfloat16).at[slot]]
    convert_element_type x3 -> x0, local copies, waits for them, and re-layouts: 5.35 us -> none  [the longest x2 2.98 us: on_device(): summed[:, 0].astype(jnp.bfloat16)]
  transfers between devices with their start and end apart: 6 -> 8, of which waited for: 4 -> 6; matrix products, arithmetic and copies ran while one was open for 2% -> 13% of each run, Pallas kernels for 0% -> 0%
where the time goes in v1:
time: 97.7 us; the launch traced here: 97.2 us
  blocking collectives  35.7 us (37%)
  waiting for transfers between devices  28.6 us (29%)
  matrix products  11.4 us (12%)
  starting transfers between devices  11.3 us (12%)
  other arithmetic  7.07 us (7%)
  local copies, waits for them, and re-layouts  2.75 us (3%)
    ppermute x6, waiting for transfers between devices, flipped(): lax.ppermute(block, axis, [(i, i ^ bit) for i in range(lax.axis_size(axis...  22.7 us
    all_to_all x1, blocking collectives, route_by_group(): lax.all_to_all(outgoing, 'sp', split_axis=0, concat_axis=0, tiled=True)  18.7 us
    all_to_all x1, blocking collectives, route_by_group(): lax.all_to_all(summed, 'sp', split_axis=0, concat_axis=0, tiled=True)  17 us
    all_to_all x1, waiting for transfers between devices, project(): lax.all_to_all(mixed, 'tp', split_axis=0, concat_axis=1, tiled=True)  5.94 us
    ppermute x1, starting transfers between devices, shifted(): return lax.ppermute(block, axis, route)  4.96 us
    all_to_all x1, starting transfers between devices, project(): lax.all_to_all(mixed, 'tp', split_axis=0, concat_axis=1, tiled=True)  3.41 us
    dot_general x1, matrix products, project(): jnp.dot(token_rows, out_proj, preferred_element_type=jnp.float32)  3.01 us
    ppermute x6, starting transfers between devices, flipped(): lax.ppermute(block, axis, [(i, i ^ bit) for i in range(lax.axis_size(axis...  2.97 us
  transfers between devices with their start and end apart: 8, of which 6 were waited for; matrix products, arithmetic and copies ran while one was open for 13% of the time, Pallas kernels for 0%

profile of v1, /device:TPU:0, one launch (start us, length us, event | category | flops | bytes accessed | tf_op | source)
XLA Modules:
  0.0 97.2 jit_solution(9595113881826151975)
XLA Ops:
  0.0 0.8 slice.127
  0.8 0.7 slice.128
  1.5 5.0 %collective-permute-start = (bf16[2,512]{1,0:T(2,128)(2,1)S(1)}, bf16[2,512]{1,0:T(2,128)(2,1)S(1)}, u32[]{:S(2)}, u32[]{:S(2)}) collective-permute-start(bf16[2,512]{1,0:T(2,128)(2,1)S(1)} %pad_maximum_fusion.1), channel_id=1, source_target_pairs={{0,4},{4,8},{8,12},{1,5},{5,9},{9,13},{2,6},{6,10},{10,14},{3,7},{... | collective-permute-start | bytes 6152 | tf_op jit(solution)/shard_map/ppermute | solution.py:13
  6.5 0.7 fusion.111
  7.2 0.7 and_select_fusion.2
  7.9 0.7 and_select_fusion
  8.6 1.1 %convert_multiply_fusion = f32[512,256]{1,0:T(8,128)S(1)} fusion(bf16[512,256]{1,0:T(8,128)(2,1)} %param.12, bf16[512,256]{1,0:T(8,128)(2,1)} %param.13), kind=kLoop, calls=%fused_computation.78 | loop fusion | flops 393216 | bytes 1048576 | tf_op jit(solution)/shard_map/mul | solution.py:29
  9.7 0.7 fusion.108
  10.4 0.2 convert_reduce_fusion
  10.6 0.9 fusion.119
  11.4 0.1 copy.26
  11.6 0.0 collective-permute-done
  11.6 1.9 %fusion.62 = bf16[512,256]{1,0:T(8,128)(2,1)} fusion(f32[2,256]{1,0:T(2,128)S(1)} %convert_multiply_fusion.1, f32[512,256]{1,0:T(8,128)S(1)} %convert_multiply_fusion, bf16[512,256]{1,0:T(8,128)(2,1)} %param.14, f32[256]{0:T(256)S(1)} %bitcast.96, f32[256]{0:T(256)S(1)} %bitcast.95, f32[256]{0:T(256)S(1)} %bitcast.94), kind=kLoop, calls=%fused_computation.75 | loop fusion | flops 1310720 | bytes 1053696 | tf_op jit(solution)/shard_map/convert_element_type | solution.py:34
  13.5 3.4 %all-to-all-start = ((bf16[4,128,256]{2,1,0:T(8,128)(2,1)}), bf16[4,128,256]{2,1,0:T(8,128)(2,1)S(1)}, u32[]{:S(2)}, u32[]{:S(2)}) async-start(bf16[4,128,256]{2,1,0:T(8,128)(2,1)} %bitcast.3), calls=%async_computation | async-start | bytes 524288 | tf_op jit(solution)/shard_map/all_to_all | solution.py:38
  16.9 5.9 %all-to-all-done = bf16[4,128,256]{2,1,0:T(8,128)(2,1)S(1)} async-done(((bf16[4,128,256]{2,1,0:T(8,128)(2,1)}), bf16[4,128,256]{2,1,0:T(8,128)(2,1)S(1)}, u32[]{:S(2)}, u32[]{:S(2)}) %all-to-all-start) | async-done | bytes 262176 | tf_op jit(solution)/shard_map/all_to_all | solution.py:38
  22.8 0.2 copy.25
  23.0 0.0 copy-done.1
  23.0 0.0 copy-start.2
  23.0 3.0 %multiply_reduce_fusion = (f32[128]{0:T(128)S(1)}, f32[128,2048]{1,0:T(8,128)S(1)}) fusion(bf16[128,1024]{0,1:T(8,128)(2,1)S(1)} %bitcast.84, bf16[1024,2048]{1,0:T(8,128)(2,1)} %param.16, bf16[128,2048]{1,0:T(8,128)(2,1)S(1)} %copy-done.1), kind=kOutput, calls=%fused_computation.47 | convolution fusion | flops 537919360 | bytes 6029824 | tf_op jit(solution)/shard_map/dot_general | solution.py:39
  26.1 0.0 copy-done.2
  26.1 0.0 copy-start.4
  26.1 0.2 multiply_convert_fusion
  26.2 0.3 convolution_convert_fusion
  26.6 18.7 %all_to_all.29 = bf16[4,32,2176]{2,1,0:T(8,128)(2,1)S(1)} all-to-all(bf16[4,32,2176]{2,1,0:T(8,128)(2,1)S(1)} %bitcast.93), channel_id=1, replica_groups=mesh['grp'=2,'sp'=4,'tp'=4] {'sp'}, dimensions={0} | all-to-all | bytes 1114112 | tf_op jit(solution)/shard_map/all_to_all | solution.py:65
  45.3 0.8 collective-permute-start.3
  46.1 0.0 collective-permute-start.1
  46.1 0.3 fusion.19
  46.4 0.2 fusion.104
  46.6 0.3 fusion.34
  46.9 0.0 copy-done.5
  47.0 0.3 fusion.4
  47.3 0.8 collective-permute-done.1
  48.1 0.2 fusion.102
  48.2 0.3 fusion.17
  48.6 0.3 fusion.32
  48.9 0.3 multiply_convert_fusion.5
  49.2 0.3 multiply_convert_fusion.6
  49.6 0.4 convolution_convert_fusion.2
  50.0 8.4 %collective-permute-done.3 = bf16[128,2176]{1,0:T(8,128)(2,1)S(1)} collective-permute-done((bf16[128,2176]{1,0:T(8,128)(2,1)S(1)}, bf16[128,2176]{1,0:T(8,128)(2,1)S(1)}, u32[]{:S(2)}, u32[]{:S(2)}) %collective-permute-start.3) | collective-permute-done | bytes 557088 | tf_op jit(solution)/shard_map/ppermute | solution.py:17
  58.4 0.0 collective-permute-start.4
  58.4 0.2 fusion.100
  58.6 0.6 collective-permute-start.2
  59.2 0.3 fusion.15
  59.5 0.3 multiply_convert_fusion.3
  59.9 0.5 collective-permute-done.4
  60.4 0.2 fusion.98
  60.6 0.3 fusion.13
  60.9 0.3 fusion.28
  61.3 0.3 multiply_convert_fusion.1
  61.6 0.3 multiply_convert_fusion.2
  61.9 0.4 convolution_convert_fusion.1
  62.4 0.2 collective-permute-start.5
  62.6 0.3 fusion.30
  62.9 0.3 multiply_convert_fusion.4
  63.2 1.1 %collective-permute-done.5 = bf16[128,2048]{1,0:T(8,128)(2,1)S(1)} collective-permute-done((bf16[128,2048]{1,0:T(8,128)(2,1)S(1)}, bf16[128,2048]{1,0:T(8,128)(2,1)S(1)}, u32[]{:S(2)}, u32[]{:S(2)}) %collective-permute-start.5) | collective-permute-done | bytes 524320 | tf_op jit(solution)/shard_map/ppermute | solution.py:17
  64.3 0.4 add_convert_fusion.1
  64.8 1.4 %collective-permute-start.6 = (bf16[128,2048]{1,0:T(8,128)(2,1)S(1)}, bf16[128,2048]{1,0:T(8,128)(2,1)S(1)}, u32[]{:S(2)}, u32[]{:S(2)}) collective-permute-start(bf16[128,2048]{1,0:T(8,128)(2,1)S(1)} %add_convert_fusion.1), channel_id=1, source_target_pairs={{0,2},{1,3},{2,0},{3,1},{4,6},{5,7},{6,4},{7,5},{8,10},{9,11},{10,... | collective-permute-start | bytes 1572872 | tf_op jit(solution)/shard_map/ppermute | solution.py:17
  66.2 0.3 fusion.3
  66.5 0.4 fusion.81
  67.0 0.0 collective-permute-done.2
  67.0 11.9 %collective-permute-done.6 = bf16[128,2048]{1,0:T(8,128)(2,1)S(1)} collective-permute-done((bf16[128,2048]{1,0:T(8,128)(2,1)S(1)}, bf16[128,2048]{1,0:T(8,128)(2,1)S(1)}, u32[]{:S(2)}, u32[]{:S(2)}) %collective-permute-start.6) | collective-permute-done | bytes 524320 | tf_op jit(solution)/shard_map/ppermute | solution.py:17
  78.8 0.2 add_convert_fusion
  79.0 17.0 %all_to_all.30 = bf16[4,32,2048]{2,1,0:T(8,128)(2,1)S(1)} all-to-all(bf16[4,32,2048]{2,1,0:T(8,128)(2,1)S(1)} %bitcast.82), channel_id=1, replica_groups=mesh['grp'=2,'sp'=4,'tp'=4] {'sp'}, dimensions={0} | all-to-all | bytes 1048576 | tf_op jit(solution)/shard_map/all_to_all | solution.py:89
  96.1 1.1 %fusion = bf16[128,2048]{1,0:T(8,128)(2,1)} fusion(f32[128,2048]{1,0:T(8,128)S(1)} %get-tuple-element.19, bf16[128,2048]{1,0:T(8,128)(2,1)S(1)} %bitcast.83, s32[128]{0:T(128)S(1)} %multiply_add_fusion), kind=kOutput, calls=%fused_computation.3 | convolution fusion | flops 67649536 | bytes 2097664 | tf_op jit(solution)/shard_map/dot_general | solution.py:90
  (17 shorter events, 0.1 us)
Async XLA Ops:
  0.0 49.6 %copy-start = (bf16[2,256,2048]{2,1,0:T(8,128)(2,1)S(1)}, bf16[2,256,2048]{2,1,0:T(8,128)(2,1)}, u32[]{:S(2)}) copy-start(bf16[2,256,2048]{2,1,0:T(8,128)(2,1)} %param.23) | copy-start | bytes 6291460
  0.0 16.9 %copy-start.3 = (s32[128,2]{0,1:T(2,128)S(1)}, s32[128,2]{0,1:T(2,128)}, u32[]{:S(2)}) copy-start(s32[128,2]{0,1:T(2,128)} %param.19) | copy-start | bytes 3076
  0.0 23.0 %copy-start.1 = (bf16[128,2048]{1,0:T(8,128)(2,1)S(1)}, bf16[128,2048]{1,0:T(8,128)(2,1)}, u32[]{:S(2)}) copy-start(bf16[128,2048]{1,0:T(8,128)(2,1)} %param.17) | copy-start | bytes 1572868
  1.5 10.0 %collective-permute-start = (bf16[2,512]{1,0:T(2,128)(2,1)S(1)}, bf16[2,512]{1,0:T(2,128)(2,1)S(1)}, u32[]{:S(2)}, u32[]{:S(2)}) collective-permute-start(bf16[2,512]{1,0:T(2,128)(2,1)S(1)} %pad_maximum_fusion.1), channel_id=1, source_target_pairs={{0,4},{4,8},{8,12},{1,5},{5,9},{9,13},{2,6},{6,10},{10,14},{3,7},{... | collective-permute-start | bytes 6152 | tf_op jit(solution)/shard_map/ppermute | solution.py:13
  13.5 9.4 %all-to-all-start = ((bf16[4,128,256]{2,1,0:T(8,128)(2,1)}), bf16[4,128,256]{2,1,0:T(8,128)(2,1)S(1)}, u32[]{:S(2)}, u32[]{:S(2)}) async-start(bf16[4,128,256]{2,1,0:T(8,128)(2,1)} %bitcast.3), calls=%async_computation | async-start | bytes 524288 | tf_op jit(solution)/shard_map/all_to_all | solution.py:38
  23.0 3.0 %copy-start.2 = (f32[2048]{0:T(1024)S(1)}, f32[2048]{0:T(1024)}, u32[]{:S(2)}) copy-start(f32[2048]{0:T(1024)} %param.18) | copy-start | bytes 24580
  26.1 20.0 %copy-start.4 = (bf16[2,2048,256]{2,1,0:T(8,128)(2,1)S(1)}, bf16[2,2048,256]{2,1,0:T(8,128)(2,1)}, u32[]{:S(2)}) copy-start(bf16[2,2048,256]{2,1,0:T(8,128)(2,1)} %param.21) | copy-start | bytes 6291460
  45.3 1.7 %copy-start.5 = (bf16[2,2048,256]{2,1,0:T(8,128)(2,1)S(1)}, bf16[2,2048,256]{2,1,0:T(8,128)(2,1)}, u32[]{:S(2)}) copy-start(bf16[2,2048,256]{2,1,0:T(8,128)(2,1)} %param.22) | copy-start | bytes 6291460
  45.3 13.2 %collective-permute-start.3 = (bf16[128,2176]{1,0:T(8,128)(2,1)S(1)}, bf16[128,2176]{1,0:T(8,128)(2,1)S(1)}, u32[]{:S(2)}, u32[]{:S(2)}) collective-permute-start(bf16[128,2176]{1,0:T(8,128)(2,1)S(1)} %bitcast.87), channel_id=1, source_target_pairs={{0,2},{1,3},{2,0},{3,1},{4,6},{5,7},{6,4},{7,5},{8,10},{9,11},{10,... | collective-permute-start | bytes 1671176 | tf_op jit(solution)/shard_map/ppermute | solution.py:17
  46.1 2.0 %collective-permute-start.1 = (bf16[128,2176]{1,0:T(8,128)(2,1)S(1)}, bf16[128,2176]{1,0:T(8,128)(2,1)S(1)}, u32[]{:S(2)}, u32[]{:S(2)}) collective-permute-start(bf16[128,2176]{1,0:T(8,128)(2,1)S(1)} %bitcast.88), channel_id=1, source_target_pairs={{0,1},{1,0},{2,3},{3,2},{4,5},{5,4},{6,7},{7,6},{8,9},{9,8},{10,11... | collective-permute-start | bytes 1671176 | tf_op jit(solution)/shard_map/ppermute | solution.py:17
  58.4 2.0 %collective-permute-start.4 = (bf16[128,2176]{1,0:T(8,128)(2,1)S(1)}, bf16[128,2176]{1,0:T(8,128)(2,1)S(1)}, u32[]{:S(2)}, u32[]{:S(2)}) collective-permute-start(bf16[128,2176]{1,0:T(8,128)(2,1)S(1)} %collective-permute-done.3), channel_id=1, source_target_pairs={{0,1},{1,0},{2,3},{3,2},{4,5},{5,4},{6,7},{7,6},{8,9},{9,8},{10,11... | collective-permute-start | bytes 1671176 | tf_op jit(solution)/shard_map/ppermute | solution.py:17
  58.6 8.3 %collective-permute-start.2 = (bf16[128,2048]{1,0:T(8,128)(2,1)S(1)}, bf16[128,2048]{1,0:T(8,128)(2,1)S(1)}, u32[]{:S(2)}, u32[]{:S(2)}) collective-permute-start(bf16[128,2048]{1,0:T(8,128)(2,1)S(1)} %convolution_convert_fusion.2), channel_id=1, source_target_pairs={{0,1},{1,0},{2,3},{3,2},{4,5},{5,4},{6,7},{7,6},{8,9},{9,8},{10,11... | collective-permute-start | bytes 1572872 | tf_op jit(solution)/shard_map/ppermute | solution.py:17
  62.4 2.0 %collective-permute-start.5 = (bf16[128,2048]{1,0:T(8,128)(2,1)S(1)}, bf16[128,2048]{1,0:T(8,128)(2,1)S(1)}, u32[]{:S(2)}, u32[]{:S(2)}) collective-permute-start(bf16[128,2048]{1,0:T(8,128)(2,1)S(1)} %convolution_convert_fusion.1), channel_id=1, source_target_pairs={{0,1},{1,0},{2,3},{3,2},{4,5},{5,4},{6,7},{7,6},{8,9},{9,8},{10,11... | collective-permute-start | bytes 1572872 | tf_op jit(solution)/shard_map/ppermute | solution.py:17
  64.8 14.0 %collective-permute-start.6 = (bf16[128,2048]{1,0:T(8,128)(2,1)S(1)}, bf16[128,2048]{1,0:T(8,128)(2,1)S(1)}, u32[]{:S(2)}, u32[]{:S(2)}) collective-permute-start(bf16[128,2048]{1,0:T(8,128)(2,1)S(1)} %add_convert_fusion.1), channel_id=1, source_target_pairs={{0,2},{1,3},{2,0},{3,1},{4,6},{5,7},{6,4},{7,5},{8,10},{9,11},{10,... | collective-permute-start | bytes 1572872 | tf_op jit(solution)/shard_map/ppermute | solution.py:17
